TPU v7x, 32 devices: a whole 2x2x4 slice. The times are simulated.
32 devices in a mesh: fs: 8 (over z, core), tp: 4 (over y, x).
Axes of the slice: x: 2, y: 2, z: 4, core: 2. Of those that a mesh axis runs over, the one named last changes fastest.
Arguments:
- prompt: bfloat16 [1024, 2048], P('tp'), may hold values from -6 to 6
- norm_gain: float32 [2048], P('fs'), may hold values from 0.1 to 1.9
- gate_master: float32 [32, 2048, 512], P(None, 'fs', 'tp'), may hold values from -6 to 6
- up_master: float32 [32, 2048, 512], P(None, 'fs', 'tp'), may hold values from -6 to 6
- down_master: float32 [32, 2048, 512], P(None, 'fs', 'tp'), may hold values from -6 to 6
- group_choice: int32 [1024], P('tp'), may hold values from 0 to 3
- inner_choice: int32 [1024, 2], P('tp'), may hold values from 0 to 7, as said below
- route_weight: float32 [1024, 2], P('tp'), may hold values from 0.2 to 1
Outputs:
- gate_served: bfloat16 [2048, 16384], P(None, 'fs')
- up_served: bfloat16 [2048, 16384], P(None, 'fs')
- down_served: bfloat16 [2048, 16384], P(None, 'fs')
- mixed: bfloat16 [1024, 2048], P('tp', 'fs')
Inputs may be any that keep to these rules, and one draw needn't show every extreme that they name: `inner_choice`: the two experts of a token differ.
All inputs are finite; a program needn't handle non-finite values.
Results may differ from a plain program's by a relative error of at most 0.0081.
Values may be sent and summed in bfloat16 or wider, within the bound.
A program may use at most 128 MiB of HBM per device.

v0:
```python
import jax
import jax.numpy as jnp
from jax import lax
from jax.sharding import PartitionSpec as P

FF = 512
GROUPS = 4
EPG = 8


def flatten_rows(piece):
    count, experts, rows, hidden = piece.shape
    return piece.transpose(0, 2, 1, 3).reshape(count, rows, experts * hidden)


def restore_rows(gathered, rows):
    parts = lax.axis_size("tp")
    count, total, width = gathered.shape
    blocks = total // (parts * rows)
    ordered = gathered.reshape(count, parts, blocks, rows, width).transpose(0, 2, 1, 3, 4)
    return ordered.reshape(count, total, width)


def activations(normed, gate_local, up_local, column_weight):
    width = normed.shape[1]
    gate_act = jnp.dot(normed, gate_local, preferred_element_type=jnp.float32) * width ** (-0.5)
    up_act = jnp.dot(normed, up_local, preferred_element_type=jnp.float32) * width ** (-0.5)
    return (column_weight * jax.nn.silu(gate_act) * up_act).astype(jnp.bfloat16)


def route_columns(weight, columns, experts):
    first = lax.axis_index("fs") * columns
    owner = (first + jnp.arange(columns, dtype=jnp.int32)) // FF
    onehot = (owner[None, :] == jnp.arange(experts, dtype=jnp.int32)[:, None]).astype(jnp.float32)
    return jnp.dot(weight, onehot, precision=lax.Precision.HIGHEST)


def shards(
    prompt, norm_gain, gate_master, up_master, down_master, group_choice, inner_choice, route_weight
):
    experts = GROUPS * EPG
    scale = norm_gain[None, :, None]
    gate_cast = (gate_master * scale).astype(jnp.bfloat16)
    up_cast = (up_master * scale).astype(jnp.bfloat16)
    down_cast = down_master.astype(jnp.bfloat16)
    rows = gate_master.shape[1] // lax.axis_size("tp")
    values = prompt.astype(jnp.float32)
    normed = (values * lax.rsqrt(jnp.mean(values * values, axis=1, keepdims=True) + 1e-06)).astype(
        jnp.bfloat16
    )
    chosen = group_choice[:, None] * EPG + inner_choice
    member = (chosen[:, :, None] == jnp.arange(experts, dtype=jnp.int32)[None, None, :]).astype(
        jnp.float32
    )
    weight = jnp.sum(member * route_weight[:, :, None], axis=1)
    stacked = jnp.stack([gate_cast, up_cast, down_cast])
    widened = lax.all_to_all(stacked, "tp", split_axis=2, concat_axis=3, tiled=True)
    moved = lax.all_to_all(flatten_rows(widened), "fs", split_axis=2, concat_axis=1, tiled=True)
    served = restore_rows(lax.all_gather(moved, "tp", axis=1, tiled=True), rows)
    gate_local, up_local, down_local = (served[0], served[1], served[2])
    column_weight = route_columns(weight, gate_local.shape[1], experts)
    scaled = activations(normed, gate_local, up_local, column_weight)
    summed = lax.psum_scatter(
        lax.dot_general(
            down_local, scaled, (((1,), (1,)), ((), ())), preferred_element_type=jnp.float32
        ),
        "fs",
        scatter_dimension=0,
        tiled=True,
    )
    mixed = (summed * FF ** (-0.5)).T.astype(jnp.bfloat16)
    return (gate_local, up_local, down_local, mixed)


def solution(mesh):
    in_specs = (
        P("tp", None),
        P("fs"),
        P(None, "fs", "tp"),
        P(None, "fs", "tp"),
        P(None, "fs", "tp"),
        P("tp"),
        P("tp", None),
        P("tp", None),
    )
    out_specs = (P(None, "fs"), P(None, "fs"), P(None, "fs"), P("tp", "fs"))
    return jax.shard_map(shards, mesh=mesh, in_specs=in_specs, out_specs=out_specs, check_vma=False)
```

profile of v0, /device:TPU:0, one launch (start us, length us, event | category | flops | bytes accessed | tf_op | source)
XLA Modules:
  0.0 666.3 jit_solution(537520447581431105)
XLA Ops:
  7.2 0.0 copy-start.4
  7.2 0.0 all-gather.2.cloned.1.call-start
  7.2 0.0 copy-start
  7.2 4.8 copy.90
  12.0 0.0 copy-done.4
  12.0 0.0 copy-done
  12.0 9.9 %fusion.6 = (bf16[1,32,256,128]{3,1,0,2:T(8,128)(2,1)S(1)}, bf16[1,32,256,128]{3,1,0,2:T(8,128)(2,1)S(1)}) fusion(f32[32,256,128]{2,1,0:T(8,128)S(1)} %copy-done, f32[256]{0:T(256)S(1)} %copy-done.4, f32[32,256,128]{2,1,0:T(8,128)} %param.11), kind=kLoop, calls=%fused_computation.16 | loop fusion | flops 4194304 | bytes 12583936 | tf_op jit(solution)/shard_map/stack | solution.py:56
  22.0 0.8 pad_maximum_fusion
  22.7 75.3 %all_to_all.36 = bf16[3,32,256,128]{3,1,0,2:T(8,128)(2,1)S(1)} all-to-all(bf16[3,32,256,128]{3,1,0,2:T(8,128)(2,1)S(1)} %pad_maximum_fusion), channel_id=1, replica_groups=mesh['fs'=8,'tp'=4] {'tp'}, dimensions={2} | all-to-all | bytes 12582912 | tf_op jit(solution)/shard_map/all_to_all | solution.py:57
  98.0 7.6 %copy.89 = bf16[3,32,4,64,128]{4,2,3,1,0:T(4,128)(2,1)} copy(bf16[3,32,4,64,128]{4,1,0,3,2:T(8,128)(2,1)S(1)} %bitcast.37) | data formatting | bytes 12582912 | tf_op jit(solution)/shard_map/all_to_all | solution.py:57
  105.6 10.1 %all_to_all.29 = bf16[3,32,64,512]{3,2,1,0:T(8,128)(2,1)} reshape(bf16[3,32,64,4,128]{4,3,2,1,0:T(4,128)(2,1)} %bitcast.38) | data formatting | bytes 12582912 | tf_op jit(solution)/shard_map/all_to_all | solution.py:57
  115.7 22.5 %copy.71 = bf16[3,64,32,512]{1,0,3,2:T(4,128)(2,1)} copy(bf16[3,64,32,512]{3,1,2,0:T(8,128)(2,1)} %bitcast.40) | data formatting | bytes 12582912 | tf_op jit(solution)/shard_map/reshape | solution.py:13
  138.3 15.3 %reshape.55 = bf16[8,2,196608]{2,1,0:T(2,128)(2,1)} reshape(bf16[16384,3,64]{2,1,0:T(4,128)(2,1)} %bitcast.34) | data formatting | bytes 12582912
  153.6 144.3 %all_to_all.37 = bf16[8,2,196608]{2,1,0:T(2,128)(2,1)} all-to-all(bf16[8,2,196608]{2,1,0:T(2,128)(2,1)} %reshape.55), channel_id=1, replica_groups=mesh['fs'=8,'tp'=4] {'fs'}, dimensions={0} | all-to-all | bytes 12582912 | tf_op jit(solution)/shard_map/all_to_all | solution.py:58
  297.8 14.2 %reshape.56 = bf16[16384,3,64]{2,1,0:T(4,128)(2,1)} reshape(bf16[8,2,196608]{2,1,0:T(2,128)(2,1)} %all_to_all.37) | data formatting | bytes 12582912
  312.0 23.2 %copy.73 = bf16[3,64,8,2048]{3,1,2,0:T(8,128)(2,1)} copy(bf16[3,64,8,2048]{1,0,3,2:T(4,128)(2,1)} %bitcast.35) | data formatting | bytes 12582912 | tf_op jit(solution)/shard_map/all_to_all | solution.py:58
  335.3 0.0 copy-start.5
  335.3 0.0 copy-start.3
  335.3 0.0 copy-start.2
  335.3 0.0 copy-start.1
  335.3 0.0 all-gather.2.cloned.1.call-update
  335.3 0.3 reduce-scatter.2.cloned.1.call-start
  335.6 0.3 copy-done.5
  336.0 0.0 copy-done.3
  336.0 0.0 copy-done.2
  336.0 0.5 copy-done.1
  336.5 0.3 fusion.4
  336.8 223.6 %all-gather.2.cloned.1.call-done = bf16[3,2048,2048]{2,1,0:T(8,128)(2,1)} async-done(((bf16[3,512,2048]{2,1,0:T(8,128)(2,1)}), bf16[3,2048,2048]{2,1,0:T(8,128)(2,1)}) %all-gather.2.cloned.1.call-update) | async-done | bytes 25165840 | tf_op jit(solution)/shard_map/all_gather | solution.py:59
  560.4 16.8 %fusion.20 = (bf16[1,8,4,64,2048]{4,3,1,2,0:T(8,128)(2,1)}, bf16[1,8,4,64,2048]{4,3,1,2,0:T(8,128)(2,1)}, bf16[1,8,4,64,2048]{4,3,1,2,0:T(8,128)(2,1)}) fusion(bf16[3,8,4,64,2048]{4,3,1,2,0:T(8,128)(2,1)} %bitcast.36), kind=kLoop, calls=%fused_computation.39 | loop fusion | bytes 50331648 | tf_op jit(solution)/shard_map/slice | solution.py:60
  577.2 8.4 %copy.67 = bf16[1,8,4,64,2048]{4,3,2,1,0:T(8,128)(2,1)} copy(bf16[1,8,4,64,2048]{4,3,1,2,0:T(8,128)(2,1)} %get-tuple-element.30) | data formatting | bytes 16777216 | tf_op jit(solution)/shard_map/slice | solution.py:60
  585.7 8.4 %copy.68 = bf16[1,8,4,64,2048]{4,3,2,1,0:T(8,128)(2,1)} copy(bf16[1,8,4,64,2048]{4,3,1,2,0:T(8,128)(2,1)} %get-tuple-element.29) | data formatting | bytes 16777216 | tf_op jit(solution)/shard_map/slice | solution.py:60
  594.1 8.4 %copy.69 = bf16[1,8,4,64,2048]{4,3,2,1,0:T(8,128)(2,1)} copy(bf16[1,8,4,64,2048]{4,3,1,2,0:T(8,128)(2,1)} %get-tuple-element.28) | data formatting | bytes 16777216 | tf_op jit(solution)/shard_map/slice | solution.py:60
  602.5 5.8 convolution_multiply_fusion.1
  608.3 1.4 convolution_multiply_fusion.2
  609.7 11.8 %fusion.14 = f32[2048,256]{1,0:T(8,128)} fusion(bf16[2048,2048]{1,0:T(8,128)(2,1)} %bitcast.45, f32[256,2048]{1,0:T(8,128)S(1)} %convolution_multiply_fusion.2, bf16[2048,2048]{1,0:T(8,128)(2,1)} %bitcast.43, bf16[256,2048]{1,0:T(8,128)(2,1)S(1)} %copy-done.1, f32[256]{0:T(256)S(1)} %add_rsqrt_fusion), kind=kOutput, calls=%fused_computation.23 | convolution fusion | flops 4298113024 | bytes 22021120 | tf_op jit(solution)/shard_map/dot_general | solution.py:64
  621.5 0.0 reduce-scatter.2.cloned.1.call-update
  621.5 36.2 %reduce-scatter.2.cloned.1.call-done = f32[256,256]{1,0:T(8,128)} async-done(((f32[2048,256]{1,0:T(8,128)}), f32[256,256]{1,0:T(8,128)}) %reduce-scatter.2.cloned.1.call-update) | async-done | bytes 262160 | tf_op jit(solution)/shard_map/reduce_scatter | solution.py:63
  657.7 1.0 fusion.11
  658.7 0.8 copy.70
  (5 shorter events, 0.0 us)
Async XLA Ops:
  7.2 4.8 copy-start.4
  7.2 553.3 %all-gather.2.cloned.1.call-start = ((), (), s32[]{:S(2)}) async-start(), calls=%async_computation.3 | async-start | bytes 31457280 | tf_op jit(solution)/shard_map/all_gather | solution.py:59
  7.2 4.8 copy-start
  335.3 0.7 copy-start.5
  335.3 0.7 copy-start.3
  335.3 0.7 copy-start.2
  335.3 1.3 copy-start.1
  335.3 322.4 %reduce-scatter.2.cloned.1.call-start = ((), (), s32[]{:S(2)}) async-start(), calls=%async_computation.4 | async-start | bytes 2359296 | tf_op jit(solution)/shard_map/reduce_scatter | solution.py:63
Sparse Core Ops, SparseCore 0:
  335.4 224.9 all-gather.1
  621.7 35.9 reduce-scatter.1
where the time goes:
time: 669 us; the launch traced here: 666 us
  waiting for transfers between devices  260 us (39%)
  blocking collectives  220 us (33%)
  local copies, waits for them, and re-layouts  142 us (21%)
  matrix products  19 us (3%)
  between operations  14.1 us (2%)
  other arithmetic  12 us (2%)
    all_gather x1, waiting for transfers between devices, shards(): served = restore_rows(lax.all_gather(moved, 'tp', axis=1, tiled=True), rows)  224 us
    all_to_all x1, blocking collectives, shards(): lax.all_to_all(flatten_rows(widened), 'fs', split_axis=2, concat_axis=1,...  144 us
    all_to_all x1, blocking collectives, shards(): lax.all_to_all(stacked, 'tp', split_axis=2, concat_axis=3, tiled=True)  75.3 us
    slice x4, local copies, waits for them, and re-layouts, shards(): gate_local, up_local, down_local = (served[0], served[1], served[2])  42.1 us
    reduce_scatter x1, waiting for transfers between devices, shards(): lax.psum_scatter(lax.dot_general(down_local, scaled, (((1,), (1,)), ((),...  36.2 us
    unnamed x16, local copies, waits for them, and re-layouts  36 us
    all_to_all x1, local copies, waits for them, and re-layouts, shards(): lax.all_to_all(flatten_rows(widened), 'fs', split_axis=2, concat_axis=1,...  23.2 us
    reshape x1, local copies, waits for them, and re-layouts, flatten_rows(): return piece.transpose(0, 2, 1, 3).reshape(count, rows, experts * hidden)  22.5 us
  transfers between devices with their start and end apart: 2, of which 2 were waited for; matrix products, arithmetic and copies ran while one was open for 0% of the time, Pallas kernels for 0%

commit v1 on v0

--- a/solution.py
+++ b/solution.py
@@ -1,8 +1,13 @@
+import functools
+
 import jax
 import jax.numpy as jnp
 from jax import lax
+from jax.experimental import pallas as pl
+from jax.experimental.pallas import tpu as pltpu
 from jax.sharding import PartitionSpec as P
 
+MESH = pl.DeviceIdType.MESH
 FF = 512
 GROUPS = 4
 EPG = 8
@@ -72,6 +77,224 @@
     return (gate_local, up_local, down_local, mixed)
 
 
+def cast_body(scale_ref, gate_ref, up_ref, down_ref, out_ref):
+    scale = scale_ref[...][None]
+    out_ref[0, 0] = (gate_ref[0] * scale).astype(jnp.bfloat16)
+    out_ref[1, 0] = (up_ref[0] * scale).astype(jnp.bfloat16)
+    out_ref[2, 0] = down_ref[0].astype(jnp.bfloat16)
+
+
+def cast_masters(norm_gain, gate_master, up_master, down_master, groups):
+    experts, rows, hidden = gate_master.shape
+    per = experts // groups
+    views = [part.reshape(groups, per, rows, hidden) for part in (gate_master, up_master, down_master)]
+    scale = jnp.broadcast_to(norm_gain[:, None], (rows, hidden))
+    block = pl.BlockSpec((1, per, rows, hidden), lambda i: (i, 0, 0, 0))
+    return pl.pallas_call(
+        cast_body,
+        grid=(groups,),
+        in_specs=[pl.BlockSpec((rows, hidden), lambda i: (0, 0)), block, block, block],
+        out_specs=pl.BlockSpec((3, 1, per, rows, hidden), lambda i: (0, i, 0, 0, 0)),
+        out_shape=jax.ShapeDtypeStruct((3, groups, per, rows, hidden), jnp.bfloat16),
+        name="cast",
+    )(scale, *views)
+
+
+def spread_body(groups, cast_ref, staged_ref, own, own_in, own_out, zs, zr, xs, xr, ys, yr, fxs, fxr, fys, fyr):
+    f, t = lax.axis_index("fs"), lax.axis_index("tp")
+    tx, ty, td = jnp.bitwise_xor(t, 1), jnp.bitwise_xor(t, 2), jnp.bitwise_xor(t, 3)
+    half = cast_ref.shape[2] // 2
+
+    def peer(k):
+        return jnp.bitwise_xor(f, k)
+
+    def z_copy(w, k):
+        return pltpu.make_async_remote_copy(
+            src_ref=cast_ref.at[w, peer(k)],
+            dst_ref=staged_ref.at[w, t, f],
+            send_sem=zs.at[w, k],
+            recv_sem=zr.at[w, k],
+            device_id={"fs": peer(k), "tp": t},
+            device_id_type=MESH,
+        )
+
+    def z_arrival(w, k):
+        return pltpu.make_async_remote_copy(
+            src_ref=cast_ref.at[w, peer(k)],
+            dst_ref=staged_ref.at[w, t, peer(k)],
+            send_sem=zs.at[w, k],
+            recv_sem=zr.at[w, k],
+            device_id={"fs": peer(k), "tp": t},
+            device_id_type=MESH,
+        )
+
+    def side_copy(w, k, origin, target, send, recv):
+        block = staged_ref.at[w, origin, peer(k)]
+        source = cast_ref.at[w, f] if k == 0 and origin is t else block
+        return pltpu.make_async_remote_copy(
+            src_ref=source,
+            dst_ref=block,
+            send_sem=send.at[w, k],
+            recv_sem=recv.at[w, k],
+            device_id={"fs": f, "tp": target},
+            device_id_type=MESH,
+        )
+
+    def half_copy(w, k, origin, part, target, send, recv):
+        block = staged_ref.at[w, origin, peer(k), pl.ds(part * half, half)]
+        return pltpu.make_async_remote_copy(
+            src_ref=block,
+            dst_ref=block,
+            send_sem=send.at[w, k],
+            recv_sem=recv.at[w, k],
+            device_id={"fs": f, "tp": target},
+            device_id_type=MESH,
+        )
+
+    def forward(w, k):
+        side_copy(w, k, tx, tx, xs, xr).wait_recv()
+        half_copy(w, k, tx, 0, ty, fys, fyr).start()
+        side_copy(w, k, ty, ty, ys, yr).wait_recv()
+        half_copy(w, k, ty, 1, tx, fxs, fxr).start()
+
+    barrier = pltpu.get_barrier_semaphore()
+    for k in range(1, groups):
+        pl.semaphore_signal(barrier, inc=1, device_id={"fs": peer(k), "tp": t}, device_id_type=MESH)
+    for other in (tx, ty):
+        pl.semaphore_signal(barrier, inc=1, device_id={"fs": f, "tp": other}, device_id_type=MESH)
+    pl.semaphore_wait(barrier, groups + 1)
+
+    for k in range(1, groups):
+        z_copy(0, k).start()
+
+    def one_array(w, carry):
+        for k in range(groups):
+            if k > 0:
+                z_arrival(w, k).wait_recv()
+            side_copy(w, k, t, tx, xs, xr).start()
+            side_copy(w, k, t, ty, ys, yr).start()
+            if k > 0:
+
+                @pl.when(w < 2)
+                def _():
+                    z_copy(w + 1, k).start()
+
+                forward(w, k - 1)
+            else:
+
+                @pl.when(w > 0)
+                def _():
+                    forward(w - 1, groups - 1)
+
+                pltpu.make_async_copy(cast_ref.at[w, f], own.at[w], own_in.at[w]).start()
+            if k == 1:
+                pltpu.make_async_copy(cast_ref.at[w, f], own.at[w], own_in.at[w]).wait()
+                pltpu.make_async_copy(own.at[w], staged_ref.at[w, t, f], own_out.at[w]).start()
+        return carry
+
+    lax.fori_loop(0, 3, one_array, 0)
+    forward(2, groups - 1)
+
+    def finish(w, carry):
+        pltpu.make_async_copy(own.at[w], staged_ref.at[w, t, f], own_out.at[w]).wait()
+        for k in range(groups):
+            if k > 0:
+                z_copy(w, k).wait_send()
+            side_copy(w, k, t, tx, xs, xr).wait_send()
+            side_copy(w, k, t, ty, ys, yr).wait_send()
+            half_copy(w, k, tx, 0, ty, fys, fyr).wait_send()
+            half_copy(w, k, ty, 1, tx, fxs, fxr).wait_send()
+            half_copy(w, k, td, 0, ty, fys, fyr).wait_recv()
+            half_copy(w, k, td, 1, tx, fxs, fxr).wait_recv()
+        return carry
+
+    lax.fori_loop(0, 3, finish, 0)
+
+
+def spread(cast, parts):
+    arrays, groups, per, rows, hidden = cast.shape
+    return pl.pallas_call(
+        functools.partial(spread_body, groups),
+        in_specs=[pl.BlockSpec(memory_space=pl.ANY)],
+        out_specs=pl.BlockSpec(memory_space=pl.ANY),
+        out_shape=jax.ShapeDtypeStruct((arrays, parts, groups, per, rows, hidden), cast.dtype),
+        scratch_shapes=[
+            pltpu.VMEM((arrays, per, rows, hidden), cast.dtype),
+            pltpu.SemaphoreType.DMA((arrays,)),
+            pltpu.SemaphoreType.DMA((arrays,)),
+        ]
+        + [pltpu.SemaphoreType.DMA((arrays, groups))] * 10,
+        compiler_params=pltpu.CompilerParams(collective_id=0, has_side_effects=True),
+        name="spread",
+    )(cast)
+
+
+def serve_body(normed_ref, weight_ref, staged_ref, gate_ref, up_ref, down_ref, part_ref):
+    _, parts, groups, _, rows, hidden = staged_ref.shape
+    for w, out in enumerate((gate_ref, up_ref, down_ref)):
+        for t in range(parts):
+            out[:, t * hidden : (t + 1) * hidden] = staged_ref[w, t, :, 0].reshape(groups * rows, hidden)
+    normed = normed_ref[...]
+    scaled = activations(normed, gate_ref[...], up_ref[...], weight_ref[0])
+    part = lax.dot_general(
+        scaled, down_ref[...], (((1,), (1,)), ((), ())), preferred_element_type=jnp.float32
+    )
+
+    @pl.when(pl.program_id(0) == 0)
+    def _():
+        part_ref[...] = part
+
+    @pl.when(pl.program_id(0) > 0)
+    def _():
+        part_ref[...] += part
+
+
+def serve(normed, weight, staged):
+    arrays, parts, groups, per, rows, hidden = staged.shape
+    tokens, width = normed.shape
+    out = jax.ShapeDtypeStruct((width, per * parts * hidden), staged.dtype)
+    block = pl.BlockSpec((width, parts * hidden), lambda e: (0, e))
+    return pl.pallas_call(
+        serve_body,
+        grid=(per,),
+        in_specs=[
+            pl.BlockSpec((tokens, width), lambda e: (0, 0)),
+            pl.BlockSpec((1, tokens, 1), lambda e: (e, 0, 0)),
+            pl.BlockSpec((arrays, parts, groups, 1, rows, hidden), lambda e: (0, 0, 0, e, 0, 0)),
+        ],
+        out_specs=[block, block, block, pl.BlockSpec((tokens, width), lambda e: (0, 0))],
+        out_shape=[out, out, out, jax.ShapeDtypeStruct((tokens, width), jnp.float32)],
+        compiler_params=pltpu.CompilerParams(vmem_limit_bytes=60 * 1024 * 1024),
+        name="serve",
+    )(normed, weight, staged)
+
+
+def direct_shards(
+    prompt, norm_gain, gate_master, up_master, down_master, group_choice, inner_choice, route_weight
+):
+    groups, parts = lax.axis_size("fs"), lax.axis_size("tp")
+    per = gate_master.shape[0] // groups
+    staged = spread(cast_masters(norm_gain, gate_master, up_master, down_master, groups), parts)
+    values = prompt.astype(jnp.float32)
+    normed = (values * lax.rsqrt(jnp.mean(values * values, axis=1, keepdims=True) + 1e-06)).astype(
+        jnp.bfloat16
+    )
+    chosen = group_choice[:, None] * EPG + inner_choice
+    mine = lax.axis_index("fs") * per + jnp.arange(per, dtype=jnp.int32)
+    member = (chosen[None] == mine[:, None, None]).astype(jnp.float32)
+    weight = jnp.sum(member * route_weight[None], axis=2)[:, :, None]
+    gate_local, up_local, down_local, part = serve(normed, weight, staged)
+    summed = lax.psum_scatter(part, "fs", scatter_dimension=1, tiled=True)
+    mixed = (summed * FF ** (-0.5)).astype(jnp.bfloat16)
+    return (gate_local, up_local, down_local, mixed)
+
+
+def fits_direct(mesh):
+    groups, parts = mesh.shape["fs"], mesh.shape["tp"]
+    whole_experts = (GROUPS * EPG) % groups == 0 and (GROUPS * EPG // groups) % 2 == 0
+    return parts == 4 and groups & (groups - 1) == 0 and whole_experts and FF // parts % 128 == 0
+
+
 def solution(mesh):
     in_specs = (
         P("tp", None),
@@ -84,4 +307,5 @@
         P("tp", None),
     )
     out_specs = (P(None, "fs"), P(None, "fs"), P(None, "fs"), P("tp", "fs"))
-    return jax.shard_map(shards, mesh=mesh, in_specs=in_specs, out_specs=out_specs, check_vma=False)
+    body = direct_shards if fits_direct(mesh) else shards
+    return jax.shard_map(body, mesh=mesh, in_specs=in_specs, out_specs=out_specs, check_vma=False)

time: 669 us -> 306 us (0.46)
  Pallas kernels: 0 us -> 247 us
  waiting for transfers between devices: 260 us -> 34.7 us
  blocking collectives: 220 us -> 0 us
  local copies, waits for them, and re-layouts: 142 us -> 2.46 us
  matrix products: 19 us -> 0 us
    pallas_call x0 -> x3, Pallas kernels: none -> 247 us  [the longest x1 217 us: spread(): pl.pallas_call(functools.partial(spread_body, groups), in_specs=[pl.Block...]
    all_gather x1 -> x0, waiting for transfers between devices: 224 us -> none  [shards(): served = restore_rows(lax.all_gather(moved, 'tp', axis=1, tiled=True), rows)]
    all_to_all x2 -> x0, blocking collectives: 220 us -> none  [the longest x1 144 us: shards(): lax.all_to_all(flatten_rows(widened), 'fs', split_axis=2, concat_axis=1,...]
    slice x4 -> x0, local copies, waits for them, and re-layouts: 42.1 us -> none  [shards(): gate_local, up_local, down_local = (served[0], served[1], served[2])]
    all_to_all x3 -> x0, local copies, waits for them, and re-layouts: 40.9 us -> none  [the longest x1 23.2 us: shards(): lax.all_to_all(flatten_rows(widened), 'fs', split_axis=2, concat_axis=1,...]
    unnamed x16 -> x0, local copies, waits for them, and re-layouts: 36 us -> none
    reshape x1 -> x0, local copies, waits for them, and re-layouts: 22.5 us -> none  [flatten_rows(): return piece.transpose(0, 2, 1, 3).reshape(count, rows, experts * hidden)]
    dot_general x3 -> x0, matrix products: 19 us -> none  [the longest x1 11.8 us: shards(): lax.dot_general(down_local, scaled, (((1,), (1,)), ((), ())), preferred_e...]
  transfers between devices with their start and end apart: 2 -> 1, of which waited for: 2 -> 1; matrix products, arithmetic and copies ran while one was open for 0% -> 0% of each run, Pallas kernels for 0% -> 0%
where the time goes in v1:
time: 306 us
  Pallas kernels  247 us (81%)
  waiting for transfers between devices  34.7 us (11%)
  between operations  14.1 us (5%)
  other arithmetic  7.72 us (3%)
    pallas_call x1, Pallas kernels, spread(): pl.pallas_call(functools.partial(spread_body, groups), in_specs=[pl.Block...  217 us
    reduce_scatter x1, waiting for transfers between devices, direct_shards(): summed = lax.psum_scatter(part, 'fs', scatter_dimension=1, tiled=True)  34.7 us
    pallas_call x1, Pallas kernels, serve(): pl.pallas_call(serve_body, grid=(per,), in_specs=[pl.BlockSpec((tokens, w...  20.4 us
    pallas_call x1, Pallas kernels, cast_masters(): pl.pallas_call(cast_body, grid=(groups,), in_specs=[pl.BlockSpec((rows, h...  9.38 us
  transfers between devices with their start and end apart: 1, of which 1 were waited for; matrix products, arithmetic and copies ran while one was open for 0% of the time, Pallas kernels for 0%

profile of v1, /device:TPU:0, one launch (start us, length us, event | category | flops | bytes accessed | tf_op | source)
XLA Modules:
  0.0 305.7 jit_solution(1443224579858655120)
XLA Ops:
  7.2 0.0 reduce-scatter.2.cloned.1.call-start
  7.2 0.7 broadcast_multiply_fusion
  7.9 1.5 fusion
  9.4 0.7 broadcast_add_fusion
  10.1 0.8 select_reduce_fusion
  10.9 1.0 copy.17.weight_ref
  11.9 2.4 fusion.1.normed_ref
  14.3 1.4 broadcast_in_dim.5.scale_ref
  15.8 9.4 %cast.1.cast_ref = bf16[3,8,4,256,128]{4,3,2,1,0:T(8,128)(2,1)} custom-call(f32[256,128]{1,0:T(8,128)} %broadcast_in_dim.5.scale_ref, f32[8,4,256,128]{3,2,1,0:T(8,128)} %bitcast.4, f32[8,4,256,128]{3,2,1,0:T(8,128)} %bitcast.5, f32[8,4,256,128]{3,2,1,0:T(8,128)} %bitcast.6), custom_call_target="tpu_custom_call" | custom-call | tf_op jit(solution)/shard_map/cast/pallas_call | solution.py:93
  25.2 216.9 %spread.1.staged_ref = bf16[3,4,8,4,256,128]{5,4,3,2,1,0:T(8,128)(2,1)} custom-call(bf16[3,8,4,256,128]{4,3,2,1,0:T(8,128)(2,1)} %cast.1.cast_ref), custom_call_target="tpu_custom_call" | custom-call | tf_op jit(solution)/shard_map/spread/pallas_call | solution.py:216
  242.0 20.4 %serve.1 = (bf16[2048,2048]{1,0:T(8,128)(2,1)}, bf16[2048,2048]{1,0:T(8,128)(2,1)}, bf16[2048,2048]{1,0:T(8,128)(2,1)}, f32[256,2048]{1,0:T(8,128)}) custom-call(bf16[256,2048]{1,0:T(8,128)(2,1)} %fusion.1.normed_ref, f32[4,256,1]{2,1,0:T(8,128)} %copy.17.weight_ref, bf16[3,4,8,4,256,128]{5,4,3,2,1,0:T(8,128)(2,1)} %spread.1.staged_ref), custom_call_target="tpu_custom_call" | custom-call | tf_op jit(solution)/shard_map/serve/pallas_call | solution.py:257
  262.5 0.0 reduce-scatter.2.cloned.1.call-update
  262.5 34.7 %reduce-scatter.2.cloned.1.call-done = f32[256,256]{1,0:T(8,128)} async-done(((f32[256,2048]{1,0:T(8,128)}), f32[256,256]{1,0:T(8,128)}) %reduce-scatter.2.cloned.1.call-update) | async-done | bytes 262160 | tf_op jit(solution)/shard_map/reduce_scatter | solution.py:287
  297.2 1.6 multiply_convert_fusion
  (2 shorter events, 0.0 us)
Async XLA Ops:
  7.2 290.0 %reduce-scatter.2.cloned.1.call-start = ((), (), s32[]{:S(2)}) async-start(), calls=%async_computation.1 | async-start | bytes 2359296 | tf_op jit(solution)/shard_map/reduce_scatter | solution.py:287
Sparse Core Ops, SparseCore 0:
  262.6 34.5 reduce-scatter.1

commit v2 on v1

--- a/solution.py
+++ b/solution.py
@@ -78,7 +78,8 @@
 
 
 def cast_body(scale_ref, gate_ref, up_ref, down_ref, out_ref):
-    scale = scale_ref[...][None]
+    hidden = out_ref.shape[-1]
+    scale = jnp.broadcast_to(scale_ref[...], (hidden, scale_ref.shape[1])).T[None]
     out_ref[0, 0] = (gate_ref[0] * scale).astype(jnp.bfloat16)
     out_ref[1, 0] = (up_ref[0] * scale).astype(jnp.bfloat16)
     out_ref[2, 0] = down_ref[0].astype(jnp.bfloat16)
@@ -88,19 +89,50 @@
     experts, rows, hidden = gate_master.shape
     per = experts // groups
     views = [part.reshape(groups, per, rows, hidden) for part in (gate_master, up_master, down_master)]
-    scale = jnp.broadcast_to(norm_gain[:, None], (rows, hidden))
     block = pl.BlockSpec((1, per, rows, hidden), lambda i: (i, 0, 0, 0))
     return pl.pallas_call(
         cast_body,
         grid=(groups,),
-        in_specs=[pl.BlockSpec((rows, hidden), lambda i: (0, 0)), block, block, block],
+        in_specs=[pl.BlockSpec((1, rows), lambda i: (0, 0)), block, block, block],
         out_specs=pl.BlockSpec((3, 1, per, rows, hidden), lambda i: (0, i, 0, 0, 0)),
         out_shape=jax.ShapeDtypeStruct((3, groups, per, rows, hidden), jnp.bfloat16),
         name="cast",
-    )(scale, *views)
-
-
-def spread_body(groups, cast_ref, staged_ref, own, own_in, own_out, zs, zr, xs, xr, ys, yr, fxs, fxr, fys, fyr):
+    )(norm_gain.reshape(1, rows), *views)
+
+
+def spread_body(
+    groups,
+    cast_ref,
+    prompt_ref,
+    group_ref,
+    inner_ref,
+    route_ref,
+    staged_ref,
+    mixed_ref,
+    own,
+    normed,
+    held,
+    scaled,
+    down,
+    part,
+    got,
+    own_in,
+    own_out,
+    held_sem,
+    down_sem,
+    ps,
+    pr,
+    zs,
+    zr,
+    xs,
+    xr,
+    ys,
+    yr,
+    fxs,
+    fxr,
+    fys,
+    fyr,
+):
     f, t = lax.axis_index("fs"), lax.axis_index("tp")
     tx, ty, td = jnp.bitwise_xor(t, 1), jnp.bitwise_xor(t, 2), jnp.bitwise_xor(t, 3)
     half = cast_ref.shape[2] // 2
@@ -167,6 +199,29 @@
     for k in range(1, groups):
         z_copy(0, k).start()
 
+    def diagonal_wait(w, k):
+        half_copy(w, k, td, 0, ty, fys, fyr).wait_recv()
+        half_copy(w, k, td, 1, tx, fxs, fxr).wait_recv()
+
+    def own_load(w):
+        return pltpu.make_async_copy(cast_ref.at[w, f], own.at[w], own_in.at[w])
+
+    def own_store(w):
+        return pltpu.make_async_copy(own.at[w], staged_ref.at[w, t, f], own_out.at[w])
+
+    def part_copy(k):
+        return pltpu.make_async_remote_copy(
+            src_ref=part.at[k],
+            dst_ref=got.at[k],
+            send_sem=ps.at[k],
+            recv_sem=pr.at[k],
+            device_id={"fs": peer(k), "tp": t},
+            device_id_type=MESH,
+        )
+
+    parts, _, per, rows, hidden = staged_ref.shape[1:]
+    tokens, width = prompt_ref.shape
+
     def one_array(w, carry):
         for k in range(groups):
             if k > 0:
@@ -174,11 +229,7 @@
             side_copy(w, k, t, tx, xs, xr).start()
             side_copy(w, k, t, ty, ys, yr).start()
             if k > 0:
-
-                @pl.when(w < 2)
-                def _():
-                    z_copy(w + 1, k).start()
-
+                z_copy(w + 1, k * (1 - w) + (groups - k) * w).start()
                 forward(w, k - 1)
             else:
 
@@ -186,17 +237,96 @@
                 def _():
                     forward(w - 1, groups - 1)
 
-                pltpu.make_async_copy(cast_ref.at[w, f], own.at[w], own_in.at[w]).start()
+                own_load(w).start()
             if k == 1:
-                pltpu.make_async_copy(cast_ref.at[w, f], own.at[w], own_in.at[w]).wait()
-                pltpu.make_async_copy(own.at[w], staged_ref.at[w, t, f], own_out.at[w]).start()
+                own_load(w).wait()
+                own_store(w).start()
         return carry
 
-    lax.fori_loop(0, 3, one_array, 0)
-    forward(2, groups - 1)
+    def normalise():
+        values = prompt_ref[...].astype(jnp.float32)
+        mean = jnp.mean(values * values, axis=1, keepdims=True)
+        normed[...] = (values * lax.rsqrt(mean + 1e-06)).astype(jnp.bfloat16)
+
+    def hidden_units(e, carry):
+        loads = [pltpu.make_async_copy(staged_ref.at[w, :, :, e], held.at[w], held_sem.at[w]) for w in range(2)]
+        for load in loads:
+            load.start()
+        chosen = group_ref[...] * EPG + inner_ref[...]
+        weight = jnp.sum(jnp.where(chosen == f * per + e, route_ref[...], 0.0), axis=0, keepdims=True)
+        column = jnp.broadcast_to(weight, (hidden, tokens)).T
+        for load in loads:
+            load.wait()
+
+        def one_part(i, inner):
+            gate = held[0, i].reshape(groups * rows, hidden)
+            up = held[1, i].reshape(groups * rows, hidden)
+            scaled[e, i] = activations(normed[...], gate, up, column)
+            return inner
+
+        return lax.fori_loop(0, parts, one_part, carry)
+
+    def features(k):
+        diagonal_wait(2, k)
+        if k == 0:
+            own_store(2).wait()
+        load = pltpu.make_async_copy(staged_ref.at[2, :, peer(k)], down, down_sem)
+        load.start()
+        part[k] = jnp.zeros_like(part[k])
+        load.wait()
+
+        def one_expert(e, carry):
+            left = jnp.concatenate([scaled[e, i] for i in range(parts)], axis=1)
+            right = jnp.concatenate([down[i, e] for i in range(parts)], axis=1)
+            part[k] += lax.dot_general(
+                left, right, (((1,), (1,)), ((), ())), preferred_element_type=jnp.float32
+            )
+            return carry
+
+        lax.fori_loop(0, per, one_expert, 0)
+        if k > 0:
+            part_copy(k).start()
+
+    lax.fori_loop(0, 2, one_array, 0)
+
+    order = list(range(groups - 1, -1, -1))
+    done = 0
+    for i, k in enumerate(order):
+        if k > 0:
+            z_arrival(2, k).wait_recv()
+        side_copy(2, k, t, tx, xs, xr).start()
+        side_copy(2, k, t, ty, ys, yr).start()
+        if i == 0:
+            own_load(2).start()
+            forward(1, groups - 1)
+            normalise()
+        else:
+            forward(2, order[i - 1])
+        if i == 1:
+            own_load(2).wait()
+            own_store(2).start()
+            for w in range(2):
+                own_store(w).wait()
+                for other in range(groups):
+                    diagonal_wait(w, other)
+            lax.fori_loop(0, per // 2, hidden_units, 0)
+        if i == 2:
+            lax.fori_loop(per // 2, per, hidden_units, 0)
+        while i >= 3 and done <= i - 2:
+            features(order[done])
+            done += 1
+    forward(2, order[-1])
+    while done < groups:
+        features(order[done])
+        done += 1
+
+    total = part[0]
+    for k in range(groups - 1, 0, -1):
+        part_copy(k).wait_recv()
+        total = total + got[k]
+    mixed_ref[...] = (total * FF ** (-0.5)).astype(jnp.bfloat16)
 
     def finish(w, carry):
-        pltpu.make_async_copy(own.at[w], staged_ref.at[w, t, f], own_out.at[w]).wait()
         for k in range(groups):
             if k > 0:
                 z_copy(w, k).wait_send()
@@ -204,95 +334,85 @@
             side_copy(w, k, t, ty, ys, yr).wait_send()
             half_copy(w, k, tx, 0, ty, fys, fyr).wait_send()
             half_copy(w, k, ty, 1, tx, fxs, fxr).wait_send()
-            half_copy(w, k, td, 0, ty, fys, fyr).wait_recv()
-            half_copy(w, k, td, 1, tx, fxs, fxr).wait_recv()
         return carry
 
     lax.fori_loop(0, 3, finish, 0)
-
-
-def spread(cast, parts):
+    for k in range(1, groups):
+        part_copy(k).wait_send()
+
+
+def spread(cast, prompt, group_choice, inner_choice, route_weight, parts):
     arrays, groups, per, rows, hidden = cast.shape
+    tokens, width = prompt.shape
+    vmem = pl.BlockSpec(memory_space=pltpu.VMEM)
     return pl.pallas_call(
         functools.partial(spread_body, groups),
-        in_specs=[pl.BlockSpec(memory_space=pl.ANY)],
-        out_specs=pl.BlockSpec(memory_space=pl.ANY),
-        out_shape=jax.ShapeDtypeStruct((arrays, parts, groups, per, rows, hidden), cast.dtype),
+        in_specs=[pl.BlockSpec(memory_space=pl.ANY), vmem, vmem, vmem, vmem],
+        out_specs=[pl.BlockSpec(memory_space=pl.ANY), vmem],
+        out_shape=[
+            jax.ShapeDtypeStruct((arrays, parts, groups, per, rows, hidden), cast.dtype),
+            jax.ShapeDtypeStruct((tokens, width // groups), jnp.bfloat16),
+        ],
         scratch_shapes=[
             pltpu.VMEM((arrays, per, rows, hidden), cast.dtype),
+            pltpu.VMEM((tokens, width), jnp.bfloat16),
+            pltpu.VMEM((2, parts, groups, rows, hidden), cast.dtype),
+            pltpu.VMEM((per, parts, tokens, hidden), jnp.bfloat16),
+            pltpu.VMEM((parts, per, rows, hidden), cast.dtype),
+            pltpu.VMEM((groups, tokens, rows), jnp.float32),
+            pltpu.VMEM((groups, tokens, rows), jnp.float32),
             pltpu.SemaphoreType.DMA((arrays,)),
             pltpu.SemaphoreType.DMA((arrays,)),
+            pltpu.SemaphoreType.DMA((2,)),
+            pltpu.SemaphoreType.DMA,
+            pltpu.SemaphoreType.DMA((groups,)),
+            pltpu.SemaphoreType.DMA((groups,)),
         ]
         + [pltpu.SemaphoreType.DMA((arrays, groups))] * 10,
-        compiler_params=pltpu.CompilerParams(collective_id=0, has_side_effects=True),
+        compiler_params=pltpu.CompilerParams(
+            collective_id=0, has_side_effects=True, vmem_limit_bytes=60 * 1024 * 1024
+        ),
         name="spread",
-    )(cast)
-
-
-def serve_body(normed_ref, weight_ref, staged_ref, gate_ref, up_ref, down_ref, part_ref):
+    )(cast, prompt, group_choice.reshape(1, tokens), inner_choice.T, route_weight.T)
+
+
+def serve_body(staged_ref, gate_ref, up_ref, down_ref):
     _, parts, groups, _, rows, hidden = staged_ref.shape
     for w, out in enumerate((gate_ref, up_ref, down_ref)):
         for t in range(parts):
             out[:, t * hidden : (t + 1) * hidden] = staged_ref[w, t, :, 0].reshape(groups * rows, hidden)
-    normed = normed_ref[...]
-    scaled = activations(normed, gate_ref[...], up_ref[...], weight_ref[0])
-    part = lax.dot_general(
-        scaled, down_ref[...], (((1,), (1,)), ((), ())), preferred_element_type=jnp.float32
-    )
-
-    @pl.when(pl.program_id(0) == 0)
-    def _():
-        part_ref[...] = part
-
-    @pl.when(pl.program_id(0) > 0)
-    def _():
-        part_ref[...] += part
-
-
-def serve(normed, weight, staged):
+
+
+def serve(staged):
     arrays, parts, groups, per, rows, hidden = staged.shape
-    tokens, width = normed.shape
+    width = groups * rows
     out = jax.ShapeDtypeStruct((width, per * parts * hidden), staged.dtype)
     block = pl.BlockSpec((width, parts * hidden), lambda e: (0, e))
     return pl.pallas_call(
         serve_body,
         grid=(per,),
-        in_specs=[
-            pl.BlockSpec((tokens, width), lambda e: (0, 0)),
-            pl.BlockSpec((1, tokens, 1), lambda e: (e, 0, 0)),
-            pl.BlockSpec((arrays, parts, groups, 1, rows, hidden), lambda e: (0, 0, 0, e, 0, 0)),
-        ],
-        out_specs=[block, block, block, pl.BlockSpec((tokens, width), lambda e: (0, 0))],
-        out_shape=[out, out, out, jax.ShapeDtypeStruct((tokens, width), jnp.float32)],
+        in_specs=[pl.BlockSpec((arrays, parts, groups, 1, rows, hidden), lambda e: (0, 0, 0, e, 0, 0))],
+        out_specs=[block, block, block],
+        out_shape=[out, out, out],
         compiler_params=pltpu.CompilerParams(vmem_limit_bytes=60 * 1024 * 1024),
         name="serve",
-    )(normed, weight, staged)
+    )(staged)
 
 
 def direct_shards(
     prompt, norm_gain, gate_master, up_master, down_master, group_choice, inner_choice, route_weight
 ):
     groups, parts = lax.axis_size("fs"), lax.axis_size("tp")
-    per = gate_master.shape[0] // groups
-    staged = spread(cast_masters(norm_gain, gate_master, up_master, down_master, groups), parts)
-    values = prompt.astype(jnp.float32)
-    normed = (values * lax.rsqrt(jnp.mean(values * values, axis=1, keepdims=True) + 1e-06)).astype(
-        jnp.bfloat16
-    )
-    chosen = group_choice[:, None] * EPG + inner_choice
-    mine = lax.axis_index("fs") * per + jnp.arange(per, dtype=jnp.int32)
-    member = (chosen[None] == mine[:, None, None]).astype(jnp.float32)
-    weight = jnp.sum(member * route_weight[None], axis=2)[:, :, None]
-    gate_local, up_local, down_local, part = serve(normed, weight, staged)
-    summed = lax.psum_scatter(part, "fs", scatter_dimension=1, tiled=True)
-    mixed = (summed * FF ** (-0.5)).astype(jnp.bfloat16)
+    cast = cast_masters(norm_gain, gate_master, up_master, down_master, groups)
+    staged, mixed = spread(cast, prompt, group_choice, inner_choice, route_weight, parts)
+    gate_local, up_local, down_local = serve(staged)
     return (gate_local, up_local, down_local, mixed)
 
 
 def fits_direct(mesh):
     groups, parts = mesh.shape["fs"], mesh.shape["tp"]
     whole_experts = (GROUPS * EPG) % groups == 0 and (GROUPS * EPG // groups) % 2 == 0
-    return parts == 4 and groups & (groups - 1) == 0 and whole_experts and FF // parts % 128 == 0
+    return parts == 4 and groups >= 4 and groups & (groups - 1) == 0 and whole_experts and FF // parts % 128 == 0
 
 
 def solution(mesh):

time: 306 us -> 256 us (0.84)
  waiting for transfers between devices: 34.7 us -> 0 us
  between operations: 14.1 us -> 0.65 us
  other arithmetic: 7.72 us -> 0 us
  Pallas kernels: 247 us -> 254 us
    reduce_scatter x1 -> x0, waiting for transfers between devices: 34.7 us -> none  [direct_shards(): summed = lax.psum_scatter(part, 'fs', scatter_dimension=1, tiled=True)]
    pallas_call x1, Pallas kernels: 217 us -> 228 us  [spread(): pl.pallas_call(functools.partial(spread_body, groups), in_specs=[pl.Block...]
    convert_element_type x2 -> x0, other arithmetic: 4.06 us -> none  [the longest x1 2.44 us: direct_shards(): (values * lax.rsqrt(jnp.mean(values * values, axis=1, keepdims=True) + 1e...]
    pallas_call x2, Pallas kernels: 29.8 us -> 26.4 us  [the longest x1 16.9 us: serve(): pl.pallas_call(serve_body, grid=(per,), in_specs=[pl.BlockSpec((arrays, p...]
  transfers between devices with their start and end apart: 1 -> 0, of which waited for: 1 -> 0; matrix products, arithmetic and copies ran while one was open for 0% -> 0% of each run, Pallas kernels for 0% -> 0%
where the time goes in v2:
time: 256 us; the launch traced here: 255 us
  Pallas kernels  254 us (99%)
    pallas_call x1, Pallas kernels, spread(): pl.pallas_call(functools.partial(spread_body, groups), in_specs=[pl.Block...  228 us
    pallas_call x1, Pallas kernels, serve(): pl.pallas_call(serve_body, grid=(per,), in_specs=[pl.BlockSpec((arrays, p...  16.9 us
    pallas_call x1, Pallas kernels, cast_masters(): pl.pallas_call(cast_body, grid=(groups,), in_specs=[pl.BlockSpec((1, rows...  9.51 us

profile of v2, /device:TPU:0, one launch (start us, length us, event | category | flops | bytes accessed | tf_op | source)
XLA Modules:
  0.0 255.3 jit_solution(8048194759135052647)
XLA Ops:
  0.6 9.5 %cast.1.cast_ref = bf16[3,8,4,256,128]{4,3,2,1,0:T(8,128)(2,1)} custom-call(f32[1,256]{1,0:T(1,128)} %bitcast.12, f32[8,4,256,128]{3,2,1,0:T(8,128)} %bitcast.7, f32[8,4,256,128]{3,2,1,0:T(8,128)} %bitcast.8, f32[8,4,256,128]{3,2,1,0:T(8,128)} %bitcast.9), custom_call_target="tpu_custom_call" | custom-call | tf_op jit(solution)/shard_map/cast/pallas_call | solution.py:93
  10.1 227.6 %spread.1 = (bf16[3,4,8,4,256,128]{5,4,3,2,1,0:T(8,128)(2,1)}, bf16[256,256]{1,0:T(8,128)(2,1)}) custom-call(bf16[3,8,4,256,128]{4,3,2,1,0:T(8,128)(2,1)} %cast.1.cast_ref, bf16[256,2048]{1,0:T(8,128)(2,1)} %prompt_ref.1, s32[1,256]{1,0:T(1,128)} %bitcast.13, s32[2,256]{1,0:T(2,128)} %bitcast.10, f32[2,256]{1,0:T(2,128)} %bitcast.11), custom_call_target="tpu_custom_call" | custom-call | tf_op jit(solution)/shard_map/spread/pallas_call | solution.py:348
  237.8 0.0 copy-start
  237.8 16.9 %serve.1 = (bf16[2048,2048]{1,0:T(8,128)(2,1)}, bf16[2048,2048]{1,0:T(8,128)(2,1)}, bf16[2048,2048]{1,0:T(8,128)(2,1)}) custom-call(bf16[3,4,8,4,256,128]{5,4,3,2,1,0:T(8,128)(2,1)} %get-tuple-element.9.staged_ref), custom_call_target="tpu_custom_call" | custom-call | tf_op jit(solution)/shard_map/serve/pallas_call | solution.py:391
  254.7 0.0 copy-done
  254.7 0.7 copy.13
Async XLA Ops:
  237.8 16.9 %copy-start = (bf16[256,256]{1,0:T(8,128)(2,1)S(1)}, bf16[256,256]{1,0:T(8,128)(2,1)}, u32[]{:S(2)}) copy-start(bf16[256,256]{1,0:T(8,128)(2,1)} %get-tuple-element.21) | copy-start | bytes 393220
